TPU v7x, 256 devices: a whole 4x4x8 slice. The times are simulated.
256 devices in a mesh: ep: 64 (over z, x, core), tp: 4 (over y).
Axes of the slice: x: 4, y: 4, z: 8, core: 2. Of those that a mesh axis runs over, the one named last changes fastest.
Arguments:
- queries: bfloat16 [32768, 2048], P('ep', 'tp'), may hold values from -6 to 6
- keys_values: bfloat16 [32768, 4, 128], P('ep', 'tp'), may hold values from -12 to 12
- sinks: float32 [32], P('tp'), may hold values from 1 to 5
- tokens_b: bfloat16 [32768, 2048], P(('ep', 'tp')), may hold values from -6 to 6
- norm_gain: float32 [2048], replicated, may hold values from 0.1 to 1.9
- routes: int32 [32768, 2], P(('ep', 'tp')), may hold values from 0 to 63, all different within a row; in each aligned block of 128 rows (0 to 127, 128 to 255, ...) at most 5 rows name the same one
- route_weights: float32 [32768, 2], P(('ep', 'tp')), may hold values from 0.1 to 0.9
- gate_weight: bfloat16 [64, 2048, 3584], P('ep', None, 'tp'), may hold values from -0.125 to 0.125
- up_weight: bfloat16 [64, 2048, 3584], P('ep', None, 'tp'), may hold values from -0.125 to 0.125
- down_weight: bfloat16 [64, 3584, 2048], P('ep', 'tp'), may hold values from -0.09375 to 0.09375
Outputs:
- attended: bfloat16 [32768, 2048], P('ep', 'tp')
- moe_out: bfloat16 [32768, 2048], P(('ep', 'tp'))
Inputs may be any that keep to these rules, and one draw needn't show every extreme that they name: `routes`: in each aligned block of 128 rows (the rows of one device) no expert is named by more than 5 rows; the 2 entries of a row differ.
All inputs are finite; a program needn't handle non-finite values.
Results may differ from a plain program's by a relative error of at most 0.012.
Values may be sent and summed in bfloat16 or wider, within the bound.
A program may use at most 128 MiB of HBM per device.

v0:
```python
import jax
import jax.numpy as jnp
from jax import lax
from jax.sharding import PartitionSpec as P

HEADS = 32
WINDOW = 128
NEG_SCORE = -1e30
EPSILON = 1e-06


def passed_along(value, axis, by):
    size = lax.axis_size(axis)
    pairs = [(i, i + by) for i in range(size) if 0 <= i + by < size]
    return lax.ppermute(value, axis, pairs)


def split_up(value, dim, size):
    before, after = (value.shape[:dim], value.shape[dim + 1 :])
    return jnp.moveaxis(value.reshape(*before, size, -1, *after), dim, 0)


def sent_and_summed(value, axis, dim):
    parts = split_up(value, dim, lax.axis_size(axis))
    arrived = lax.all_to_all(parts, axis, split_axis=0, concat_axis=0, tiled=True)
    return arrived.astype(jnp.float32).sum(axis=0)


def window_attention(queries, keys_values, sinks):
    row_count, kv_local, doubled = keys_values.shape
    head_size = doubled // 2
    heads_local = queries.shape[1] // head_size
    group_size = heads_local // kv_local
    window_rows = WINDOW
    block_count = row_count // window_rows
    earlier = passed_along(keys_values[row_count - window_rows :], "ep", 1)
    extended = jnp.concatenate([earlier, keys_values], axis=0)
    banded = jnp.concatenate(
        [
            extended[:row_count].reshape(block_count, window_rows, kv_local, doubled),
            extended[window_rows:].reshape(block_count, window_rows, kv_local, doubled),
        ],
        axis=1,
    )
    grouped = queries.reshape(block_count, window_rows, kv_local, group_size, head_size)
    scores = jnp.einsum(
        "nqkgd,nskd->nkgqs", grouped, banded[..., :head_size], preferred_element_type=jnp.float32
    ) * head_size ** (-0.5)
    first_head = lax.axis_index("tp") * heads_local
    head_ids = (first_head + jnp.arange(heads_local, dtype=jnp.int32)).astype(jnp.float32)
    slopes = (2.0 ** (-8.0 * (head_ids + 1.0) / HEADS)).reshape(1, kv_local, group_size, 1, 1)
    query_pos = jnp.arange(window_rows, dtype=jnp.int32)[:, None]
    key_pos = jnp.arange(2 * window_rows, dtype=jnp.int32)[None, :]
    distance = window_rows + query_pos - key_pos
    offset = lax.axis_index("ep") * row_count
    key_global = (
        offset + (jnp.arange(block_count, dtype=jnp.int32)[:, None] - 1) * window_rows + key_pos
    )
    allowed = (distance >= 0)[None] & (distance < window_rows)[None] & (key_global >= 0)[:, None, :]
    scores = jnp.where(
        allowed[:, None, None], scores - slopes * distance.astype(jnp.float32), NEG_SCORE
    )
    sink_logit = sinks.reshape(1, kv_local, group_size, 1, 1)
    peak_score = jnp.maximum(jnp.max(scores, axis=-1, keepdims=True), sink_logit)
    exponent = jnp.exp(scores - peak_score)
    denominator = jnp.sum(exponent, axis=-1, keepdims=True) + jnp.exp(sink_logit - peak_score)
    weights = (exponent / denominator).astype(jnp.bfloat16)
    mixed = jnp.einsum(
        "nkgqs,nskd->nqkgd", weights, banded[..., head_size:], preferred_element_type=jnp.float32
    )
    return mixed.astype(jnp.bfloat16).reshape(row_count, heads_local * head_size)


def slot_ranks(chosen, expert_count):
    onehot = (chosen[:, :, None] == jnp.arange(expert_count, dtype=jnp.int32)).astype(jnp.int32)
    return jnp.sum(jnp.cumsum(onehot, axis=1) * onehot, axis=2) - 1


def local(
    queries,
    keys_values,
    sinks,
    tokens_b,
    norm_gain,
    routes,
    route_weights,
    gate_weight,
    up_weight,
    down_weight,
):
    attended = window_attention(queries, keys_values, sinks)
    widened = tokens_b.astype(jnp.float32)
    scale = lax.rsqrt(jnp.mean(widened * widened, axis=-1, keepdims=True) + EPSILON)
    normed = (widened * scale * norm_gain).astype(jnp.bfloat16)
    own_rows, top_count = routes.shape
    model_width = normed.shape[1]
    expert_count = lax.axis_size("ep")
    capacity = max(2, 5 * own_rows * top_count // (4 * expert_count))
    pair_count = own_rows * top_count
    own_experts = routes.reshape(pair_count)
    gate_local = gate_weight[0]
    up_local = up_weight[0]
    own_slots = slot_ranks(own_experts[None], expert_count)[0]
    table = jnp.full((expert_count * capacity,), pair_count, jnp.int32)
    table = table.at[own_experts * capacity + own_slots].set(
        jnp.arange(pair_count, dtype=jnp.int32)
    )
    padded = jnp.concatenate([normed, jnp.zeros((1, model_width), jnp.bfloat16)], axis=0)
    outgoing = padded[table // top_count].reshape(expert_count, capacity, model_width)
    arrived = lax.all_to_all(outgoing, "ep", split_axis=0, concat_axis=0, tiled=True)
    piece = lax.all_gather(arrived, "tp", axis=0, tiled=True)
    flat_rows = piece.reshape(-1, model_width)
    gate_part = jnp.dot(flat_rows, gate_local, preferred_element_type=jnp.float32)
    up_part = jnp.dot(flat_rows, up_local, preferred_element_type=jnp.float32)
    result = (jax.nn.silu(gate_part) * up_part).astype(jnp.bfloat16)
    hidden = result.reshape(piece.shape[0], capacity, gate_local.shape[1]).reshape(
        -1, gate_local.shape[1]
    )
    down_local = down_weight[0]
    summed = sent_and_summed(
        jnp.dot(hidden, down_local, preferred_element_type=jnp.float32).astype(jnp.bfloat16),
        "tp",
        0,
    ).astype(jnp.bfloat16)
    returned = lax.all_to_all(
        summed.reshape(-1, capacity, model_width), "ep", split_axis=0, concat_axis=0, tiled=True
    )
    returned = returned.reshape(-1, model_width)
    picked = returned[own_experts * capacity + own_slots].astype(jnp.float32)
    weighted = picked.reshape(own_rows, top_count, model_width) * route_weights[:, :, None]
    moe_out = jnp.sum(weighted, axis=1).astype(jnp.bfloat16)
    return (attended, moe_out)


def solution(mesh):
    in_specs = (
        P("ep", "tp"),
        P("ep", "tp", None),
        P("tp"),
        P(("ep", "tp"), None),
        P(),
        P(("ep", "tp"), None),
        P(("ep", "tp"), None),
        P("ep", None, "tp"),
        P("ep", None, "tp"),
        P("ep", "tp", None),
    )
    out_specs = (P("ep", "tp"), P(("ep", "tp"), None))
    return jax.shard_map(local, mesh=mesh, in_specs=in_specs, out_specs=out_specs, check_vma=False)
```

profile of v0, /device:TPU:2, one launch (start us, length us, event | category | flops | bytes accessed | tf_op | source)
XLA Modules:
  0.0 333.7 jit_solution(17974118181820881681)
XLA Ops:
  7.2 0.0 all-gather.2.cloned.1.call-start
  7.2 0.8 copy.35
  8.0 0.1 eq.27
  8.1 0.1 compare_convert_fusion
  8.2 0.6 reduce-window.6
  8.8 0.2 slice_reduce_fusion
  9.0 0.1 copy.37
  9.1 0.7 broadcast_multiply_fusion.1
  9.8 0.1 copy.38
  9.9 0.1 broadcast.265
  10.0 0.1 fusion.30
  10.2 0.1 copy.34
  10.3 0.1 mul.113
  10.4 1.4 scatter_custom_fusion
  11.9 1.2 fusion.15
  13.1 1.2 fusion.17
  14.4 2.4 gather_fusion
  16.9 0.6 reshape.351
  17.4 63.1 %all_to_all.15 = bf16[64,5,2048]{2,1,0:T(8,128)(2,1)S(1)} all-to-all(bf16[64,5,2048]{2,1,0:T(8,128)(2,1)S(1)} %reshape.351), channel_id=1, replica_groups=mesh['ep'=64,'tp'=4] {'ep'}, dimensions={0} | all-to-all | bytes 2621440 | tf_op jit(solution)/shard_map/all_to_all | solution.py:110
  80.5 1.9 copy.39
  82.4 0.0 all-gather.2.cloned.1.call-update
  82.4 56.0 %all-gather.2.cloned.1.call-done = bf16[256,5,2048]{2,0,1:T(8,128)(2,1)} async-done(((bf16[64,5,2048]{2,0,1:T(8,128)(2,1)}), bf16[256,5,2048]{2,0,1:T(8,128)(2,1)}) %all-gather.2.cloned.1.call-update) | async-done | bytes 5242896 | tf_op jit(solution)/shard_map/all_gather | solution.py:111
  138.4 8.9 %copy.40 = bf16[256,5,2048]{2,1,0:T(8,128)(2,1)} copy(bf16[256,5,2048]{2,0,1:T(8,128)(2,1)} %all-gather.2.cloned.1.call-done) | data formatting | bytes 10485760 | tf_op jit(solution)/shard_map/all_gather | solution.py:111
  147.3 10.0 %reshape.352 = bf16[1280,2048]{1,0:T(8,128)(2,1)} reshape(bf16[256,5,2048]{2,1,0:T(8,128)(2,1)} %copy.40) | data formatting | bytes 10485760 | tf_op jit(solution)/shard_map/reshape | solution.py:112
  157.3 10.0 %fusion.4 = f32[1280,896]{1,0:T(8,128)} fusion(bf16[1280,2048]{1,0:T(8,128)(2,1)} %reshape.352, bf16[1,2048,896]{2,1,0:T(8,128)(2,1)} %param.17), kind=kOutput, calls=%fused_computation.12 | convolution fusion | flops 4697620480 | bytes 13500416 | tf_op jit(solution)/shard_map/dot_general | solution.py:113
  167.3 17.5 %convolution_convert_fusion = bf16[1280,2048]{1,0:T(8,128)(2,1)} fusion(bf16[1,896,2048]{2,1,0:T(8,128)(2,1)} %param.19, f32[1280,896]{1,0:T(8,128)} %fusion.4, bf16[1280,2048]{1,0:T(8,128)(2,1)} %reshape.352, bf16[1,2048,896]{2,1,0:T(8,128)(2,1)} %param.18), kind=kOutput, calls=%fused_computation.3 | convolution fusion | flops 9404743680 | bytes 22413312 | tf_op jit(solution)/shard_map/dot_general | solution.py:121
  184.8 0.0 copy-start
  184.8 5.2 %all-to-all-start.1 = ((bf16[4,320,2048]{2,1,0:T(8,128)(2,1)}), bf16[4,320,2048]{2,1,0:T(8,128)(2,1)}, u32[]{:S(2)}, u32[]{:S(2)}) async-start(bf16[4,320,2048]{2,1,0:T(8,128)(2,1)} %bitcast.85), calls=%async_computation.1 | async-start | bytes 10485760 | tf_op jit(solution)/shard_map/all_to_all | solution.py:25
  190.0 0.0 copy-done
  190.0 0.6 slice.18
  190.7 1.9 collective-permute-start
  192.6 0.1 add_compare_fusion
  192.8 0.2 broadcast_and_fusion
  193.0 57.3 %all-to-all-done.1 = bf16[4,320,2048]{2,1,0:T(8,128)(2,1)} async-done(((bf16[4,320,2048]{2,1,0:T(8,128)(2,1)}), bf16[4,320,2048]{2,1,0:T(8,128)(2,1)}, u32[]{:S(2)}, u32[]{:S(2)}) %all-to-all-start.1) | async-done | bytes 5242912 | tf_op jit(solution)/shard_map/all_to_all | solution.py:25
  250.2 3.6 %reduce_sum.51 = bf16[320,2048]{1,0:T(8,128)(2,1)S(1)} reduce(bf16[4,320,2048]{2,1,0:T(8,128)(2,1)} %all-to-all-done.1, bf16[]{:T(256)} %constant.73.clone.1), dimensions={0}, to_apply=%region_7.8 | reduce | flops 1966080 | bytes 6553602 | tf_op jit(solution)/shard_map/reduce_sum | solution.py:26
  253.9 1.6 reshape.354
  255.5 0.0 copy-start.3
  255.5 10.9 %all-to-all-start.2 = ((bf16[64,5,2048]{2,1,0:T(8,128)(2,1)}), bf16[64,5,2048]{2,1,0:T(8,128)(2,1)S(1)}, u32[]{:S(2)}, u32[]{:S(2)}) async-start(bf16[64,5,2048]{2,1,0:T(8,128)(2,1)} %reshape.354), calls=%async_computation.2 | async-start | bytes 4194304 | tf_op jit(solution)/shard_map/all_to_all | solution.py:125
  266.4 0.1 broadcast_multiply_fusion
  266.6 0.1 copy.29
  266.7 0.0 copy-start.2
  266.7 2.4 reshape.385
  269.1 0.0 copy-done.3
  269.1 0.7 copy.41
  269.8 0.0 collective-permute-done
  269.8 1.4 pad_maximum_fusion.1
  271.3 1.0 copy.28
  272.3 2.3 fusion.6
  274.6 0.0 copy-done.2
  274.6 0.1 broadcast_maximum_fusion
  274.6 1.1 fusion.1
  275.7 0.1 exponential_add_fusion
  275.8 2.1 fusion.12
  277.9 1.6 copy.48
  279.5 1.4 reshape.386
  280.9 36.8 %all-to-all-done.2 = bf16[64,5,2048]{2,1,0:T(8,128)(2,1)S(1)} async-done(((bf16[64,5,2048]{2,1,0:T(8,128)(2,1)}), bf16[64,5,2048]{2,1,0:T(8,128)(2,1)S(1)}, u32[]{:S(2)}, u32[]{:S(2)}) %all-to-all-start.2) | async-done | bytes 1310752 | tf_op jit(solution)/shard_map/all_to_all | solution.py:125
  317.6 0.6 reshape.355
  318.2 0.0 copy-start.1
  318.2 2.3 gather_fusion.1
  320.6 2.4 reshape.357
  322.9 0.0 copy-done.1
  323.0 3.9 %multiply_reduce_fusion = bf16[128,2048]{1,0:T(8,128)(2,1)} fusion(f32[128,2,2048]{2,1,0:T(2,128)S(1)} %reshape.357, f32[128,2]{1,0:T(8,128)S(1)} %copy-done.1), kind=kLoop, calls=%fused_computation.17 | loop fusion | flops 786432 | bytes 2622464 | tf_op jit(solution)/shard_map/reduce_sum | solution.py:131
  (16 shorter events, 0.2 us)
Async XLA Ops:
  7.2 131.3 %all-gather.2.cloned.1.call-start = ((), (), s32[]{:S(2)}) async-start(), calls=%async_computation.3 | async-start | bytes 6553600 | tf_op jit(solution)/shard_map/all_gather | solution.py:111
  184.8 5.2 %copy-start = (bf16[512,1,128]{2,0,1:T(8,128)(2,1)S(1)}, bf16[512,1,128]{2,0,1:T(8,128)(2,1)}, u32[]{:S(2)}) copy-start(bf16[512,1,128]{2,0,1:T(8,128)(2,1)} %param.11) | copy-start | bytes 393220
  184.8 65.4 %all-to-all-start.1 = ((bf16[4,320,2048]{2,1,0:T(8,128)(2,1)}), bf16[4,320,2048]{2,1,0:T(8,128)(2,1)}, u32[]{:S(2)}, u32[]{:S(2)}) async-start(bf16[4,320,2048]{2,1,0:T(8,128)(2,1)} %bitcast.85), calls=%async_computation.1 | async-start | bytes 10485760 | tf_op jit(solution)/shard_map/all_to_all | solution.py:25
  190.7 79.2 %collective-permute-start = (bf16[128,1,128]{2,0,1:T(8,128)(2,1)}, bf16[128,1,128]{2,0,1:T(8,128)(2,1)}, u32[]{:S(2)}, u32[]{:S(2)}) collective-permute-start(bf16[128,1,128]{2,0,1:T(8,128)(2,1)} %slice.18), channel_id=1, source_target_pairs={{0,4},{4,8},{8,12},{12,16},{16,20},{20,24},{24,28},{28,32},{32,36}... | collective-permute-start | bytes 98312 | tf_op jit(solution)/shard_map/ppermute | solution.py:15
  255.5 13.6 %copy-start.3 = (f32[128,2]{0,1:T(2,128)S(1)}, f32[128,2]{0,1:T(2,128)}, u32[]{:S(2)}) copy-start(f32[128,2]{0,1:T(2,128)} %param.16) | copy-start | bytes 3076
  255.5 62.1 %all-to-all-start.2 = ((bf16[64,5,2048]{2,1,0:T(8,128)(2,1)}), bf16[64,5,2048]{2,1,0:T(8,128)(2,1)S(1)}, u32[]{:S(2)}, u32[]{:S(2)}) async-start(bf16[64,5,2048]{2,1,0:T(8,128)(2,1)} %reshape.354), calls=%async_computation.2 | async-start | bytes 4194304 | tf_op jit(solution)/shard_map/all_to_all | solution.py:125
  266.7 7.9 %copy-start.2 = (f32[8]{0:T(128)S(1)}, f32[8]{0:T(128)}, u32[]{:S(2)}) copy-start(f32[8]{0:T(128)} %param.12) | copy-start | bytes 100
  318.2 4.7 %copy-start.1 = (f32[128,2]{1,0:T(8,128)S(1)}, f32[128,2]{1,0:T(8,128)}, u32[]{:S(2)}) copy-start(f32[128,2]{1,0:T(8,128)} %copy.41) | copy-start | bytes 3076
Sparse Core Ops, SparseCore 0:
  82.5 55.8 all-gather.1
where the time goes:
time: 335 us; the launch traced here: 334 us
  waiting for transfers between devices  150 us (45%)
  blocking collectives  63.1 us (19%)
  local copies, waits for them, and re-layouts  41.7 us (12%)
  matrix products  31.8 us (9%)
  starting transfers between devices  18 us (5%)
  other arithmetic  14.7 us (4%)
  between operations  14.3 us (4%)
    all_to_all x1, blocking collectives, local(): lax.all_to_all(outgoing, 'ep', split_axis=0, concat_axis=0, tiled=True)  63.1 us
    all_to_all x1, waiting for transfers between devices, sent_and_summed(): lax.all_to_all(parts, axis, split_axis=0, concat_axis=0, tiled=True)  57.3 us
    all_gather x1, waiting for transfers between devices, local(): piece = lax.all_gather(arrived, 'tp', axis=0, tiled=True)  56 us
    all_to_all x1, waiting for transfers between devices, local(): lax.all_to_all(summed.reshape(-1, capacity, model_width), 'ep', split_axi...  36.8 us
    dot_general x1, matrix products, local(): jnp.dot(hidden, down_local, preferred_element_type=jnp.float32)  17.5 us
    all_to_all x1, starting transfers between devices, local(): lax.all_to_all(summed.reshape(-1, capacity, model_width), 'ep', split_axi...  10.9 us
    reshape x1, local copies, waits for them, and re-layouts, local(): flat_rows = piece.reshape(-1, model_width)  10 us
    dot_general x1, matrix products, local(): jnp.dot(flat_rows, gate_local, preferred_element_type=jnp.float32)  9.96 us
  transfers between devices with their start and end apart: 4, of which 3 were waited for; matrix products, arithmetic and copies ran while one was open for 6% of the time, Pallas kernels for 0%

commit v1 on v0

--- a/solution.py
+++ b/solution.py
@@ -108,7 +108,14 @@
     padded = jnp.concatenate([normed, jnp.zeros((1, model_width), jnp.bfloat16)], axis=0)
     outgoing = padded[table // top_count].reshape(expert_count, capacity, model_width)
     arrived = lax.all_to_all(outgoing, "ep", split_axis=0, concat_axis=0, tiled=True)
-    piece = lax.all_gather(arrived, "tp", axis=0, tiled=True)
+
+    def choose_the_bands(xin):
+        formed = lax.axis_size("tp")
+        frame_out = jnp.stack(formed * [xin])
+        high = lax.all_to_all(frame_out, "tp", 0, 0)
+        return jnp.concatenate(high, axis=0)
+
+    piece = choose_the_bands(arrived)
     flat_rows = piece.reshape(-1, model_width)
     gate_part = jnp.dot(flat_rows, gate_local, preferred_element_type=jnp.float32)
     up_part = jnp.dot(flat_rows, up_local, preferred_element_type=jnp.float32)

time: 335 us -> 322 us (0.961)
  blocking collectives: 63.1 us -> 126 us
  waiting for transfers between devices: 150 us -> 91.5 us
  between operations: 14.3 us -> 0.93 us
    all_to_all x0 -> x1, blocking collectives: none -> 62.8 us  [choose_the_bands(): high = lax.all_to_all(frame_out, 'tp', 0, 0)]
    all_gather x1 -> x0, waiting for transfers between devices: 56 us -> none  [local(): piece = lax.all_gather(arrived, 'tp', axis=0, tiled=True)]
    another operation x6 -> x8, local copies, waits for them, and re-layouts: 2.67 us -> 13.4 us  [the longest x1 10 us: local(): flat_rows = piece.reshape(-1, model_width)]
    reshape x1 -> x0, local copies, waits for them, and re-layouts: 10 us -> none  [local(): flat_rows = piece.reshape(-1, model_width)]
    all_gather x1 -> x0, local copies, waits for them, and re-layouts: 8.89 us -> none  [local(): piece = lax.all_gather(arrived, 'tp', axis=0, tiled=True)]
    all_to_all x0 -> x1, local copies, waits for them, and re-layouts: none -> 6.78 us  [choose_the_bands(): high = lax.all_to_all(frame_out, 'tp', 0, 0)]
  transfers between devices with their start and end apart: 4 -> 3, of which waited for: 3 -> 2; matrix products, arithmetic and copies ran while one was open for 6% -> 6% of each run, Pallas kernels for 0% -> 0%
where the time goes in v1:
time: 322 us; the launch traced here: 321 us
  blocking collectives  126 us (39%)
  waiting for transfers between devices  91.5 us (28%)
  local copies, waits for them, and re-layouts  39.2 us (12%)
  matrix products  31.8 us (10%)
  starting transfers between devices  16.5 us (5%)
  other arithmetic  14.7 us (5%)
    all_to_all x1, blocking collectives, local(): lax.all_to_all(outgoing, 'ep', split_axis=0, concat_axis=0, tiled=True)  63.1 us
    all_to_all x1, blocking collectives, choose_the_bands(): high = lax.all_to_all(frame_out, 'tp', 0, 0)  62.8 us
    all_to_all x1, waiting for transfers between devices, sent_and_summed(): lax.all_to_all(parts, axis, split_axis=0, concat_axis=0, tiled=True)  54.8 us
    all_to_all x1, waiting for transfers between devices, local(): lax.all_to_all(summed.reshape(-1, capacity, model_width), 'ep', split_axi...  36.8 us
    dot_general x1, matrix products, local(): jnp.dot(hidden, down_local, preferred_element_type=jnp.float32)  17.5 us
    another operation x1, local copies, waits for them, and re-layouts, local(): flat_rows = piece.reshape(-1, model_width)  10 us
    dot_general x1, matrix products, local(): jnp.dot(flat_rows, gate_local, preferred_element_type=jnp.float32)  9.96 us
    all_to_all x1, starting transfers between devices, local(): lax.all_to_all(summed.reshape(-1, capacity, model_width), 'ep', split_axi...  9.4 us
  transfers between devices with their start and end apart: 3, of which 2 were waited for; matrix products, arithmetic and copies ran while one was open for 6% of the time, Pallas kernels for 0%

profile of v1, /device:TPU:2, one launch (start us, length us, event | category | flops | bytes accessed | tf_op | source)
XLA Modules:
  0.0 320.6 jit_solution(3518673461778295815)
XLA Ops:
  0.6 0.8 copy.35
  1.4 0.1 eq.27
  1.6 0.1 compare_convert_fusion
  1.6 0.6 reduce-window.6
  2.2 0.2 slice_reduce_fusion
  2.4 0.1 copy.37
  2.5 0.7 broadcast_multiply_fusion.1
  3.2 0.1 copy.38
  3.3 0.1 broadcast.267
  3.4 0.1 fusion.30
  3.6 0.1 copy.34
  3.7 0.1 mul.113
  3.9 1.4 scatter_custom_fusion
  5.3 1.2 fusion.15
  6.5 1.2 fusion.17
  7.8 2.4 gather_fusion
  10.3 0.6 reshape.350
  10.8 63.1 %all_to_all.20 = bf16[64,5,2048]{2,1,0:T(8,128)(2,1)S(1)} all-to-all(bf16[64,5,2048]{2,1,0:T(8,128)(2,1)S(1)} %reshape.350), channel_id=1, replica_groups=mesh['ep'=64,'tp'=4] {'ep'}, dimensions={0} | all-to-all | bytes 2621440 | tf_op jit(solution)/shard_map/all_to_all | solution.py:110
  73.9 0.9 copy.39
  74.7 0.7 stack.2
  75.4 62.8 %all_to_all.21 = bf16[4,64,5,2048]{3,1,2,0:T(8,128)(2,1)S(1)} all-to-all(bf16[4,64,5,2048]{3,1,2,0:T(8,128)(2,1)S(1)} %stack.2), channel_id=1, replica_groups=mesh['ep'=64,'tp'=4] {'tp'}, dimensions={0} | all-to-all | bytes 10485760 | tf_op jit(solution)/shard_map/all_to_all | solution.py:115
  138.2 6.8 %copy.40 = bf16[4,64,5,2048]{3,2,1,0:T(8,128)(2,1)} copy(bf16[4,64,5,2048]{3,1,2,0:T(8,128)(2,1)S(1)} %all_to_all.21) | data formatting | bytes 10485760 | tf_op jit(solution)/shard_map/all_to_all | solution.py:115
  145.0 10.0 %reshape_reshape.3 = bf16[1280,2048]{1,0:T(8,128)(2,1)} reshape(bf16[4,64,5,2048]{3,2,1,0:T(8,128)(2,1)} %copy.40) | data formatting | bytes 10485760 | tf_op jit(solution)/shard_map/reshape;reshape | solution.py:119
  155.0 10.0 %fusion.4 = f32[1280,896]{1,0:T(8,128)} fusion(bf16[1280,2048]{1,0:T(8,128)(2,1)} %reshape_reshape.3, bf16[1,2048,896]{2,1,0:T(8,128)(2,1)} %param.17), kind=kOutput, calls=%fused_computation.12 | convolution fusion | flops 4697620480 | bytes 13500416 | tf_op jit(solution)/shard_map/dot_general | solution.py:120
  165.0 17.5 %convolution_convert_fusion = bf16[1280,2048]{1,0:T(8,128)(2,1)} fusion(bf16[1,896,2048]{2,1,0:T(8,128)(2,1)} %param.19, f32[1280,896]{1,0:T(8,128)} %fusion.4, bf16[1280,2048]{1,0:T(8,128)(2,1)} %reshape_reshape.3, bf16[1,2048,896]{2,1,0:T(8,128)(2,1)} %param.18), kind=kOutput, calls=%fused_computation.3 | convolution fusion | flops 9404743680 | bytes 22413312 | tf_op jit(solution)/shard_map/dot_general | solution.py:128
  182.5 0.0 copy-start
  182.5 5.2 %all-to-all-start.2 = ((bf16[4,320,2048]{2,1,0:T(8,128)(2,1)}), bf16[4,320,2048]{2,1,0:T(8,128)(2,1)}, u32[]{:S(2)}, u32[]{:S(2)}) async-start(bf16[4,320,2048]{2,1,0:T(8,128)(2,1)} %bitcast.85), calls=%async_computation.2 | async-start | bytes 10485760 | tf_op jit(solution)/shard_map/all_to_all | solution.py:25
  187.7 0.0 copy-done
  187.7 0.6 slice.18
  188.3 1.9 collective-permute-start
  190.3 0.1 add_compare_fusion
  190.4 0.2 broadcast_and_fusion
  190.6 54.8 %all-to-all-done.2 = bf16[4,320,2048]{2,1,0:T(8,128)(2,1)} async-done(((bf16[4,320,2048]{2,1,0:T(8,128)(2,1)}), bf16[4,320,2048]{2,1,0:T(8,128)(2,1)}, u32[]{:S(2)}, u32[]{:S(2)}) %all-to-all-start.2) | async-done | bytes 5242912 | tf_op jit(solution)/shard_map/all_to_all | solution.py:25
  245.4 3.6 %reduce_sum.51 = bf16[320,2048]{1,0:T(8,128)(2,1)S(1)} reduce(bf16[4,320,2048]{2,1,0:T(8,128)(2,1)} %all-to-all-done.2, bf16[]{:T(256)} %constant.73.clone.1), dimensions={0}, to_apply=%region_7.8 | reduce | flops 1966080 | bytes 6553602 | tf_op jit(solution)/shard_map/reduce_sum | solution.py:26
  249.0 1.6 reshape.352
  250.7 0.0 copy-start.3
  250.7 9.4 %all-to-all-start.3 = ((bf16[64,5,2048]{2,1,0:T(8,128)(2,1)}), bf16[64,5,2048]{2,1,0:T(8,128)(2,1)S(1)}, u32[]{:S(2)}, u32[]{:S(2)}) async-start(bf16[64,5,2048]{2,1,0:T(8,128)(2,1)} %reshape.352), calls=%async_computation.3 | async-start | bytes 4194304 | tf_op jit(solution)/shard_map/all_to_all | solution.py:132
  260.1 0.1 broadcast_multiply_fusion
  260.3 0.1 copy.29
  260.4 0.0 copy-start.2
  260.4 2.4 reshape.383
  262.8 0.0 copy-done.3
  262.8 0.7 copy.41
  263.5 0.0 collective-permute-done
  263.5 1.4 pad_maximum_fusion.1
  264.9 1.0 copy.28
  266.0 2.3 fusion.6
  268.2 0.0 copy-done.2
  268.3 0.1 broadcast_maximum_fusion
  268.3 1.1 fusion.1
  269.4 0.1 exponential_add_fusion
  269.5 2.1 fusion.12
  271.6 1.6 copy.48
  273.2 1.4 reshape.384
  274.6 36.8 %all-to-all-done.3 = bf16[64,5,2048]{2,1,0:T(8,128)(2,1)S(1)} async-done(((bf16[64,5,2048]{2,1,0:T(8,128)(2,1)}), bf16[64,5,2048]{2,1,0:T(8,128)(2,1)S(1)}, u32[]{:S(2)}, u32[]{:S(2)}) %all-to-all-start.3) | async-done | bytes 1310752 | tf_op jit(solution)/shard_map/all_to_all | solution.py:132
  311.3 0.6 reshape.353
  311.9 0.0 copy-start.1
  311.9 2.3 gather_fusion.1
  314.3 2.4 reshape.355
  316.6 0.0 copy-done.1
  316.6 3.9 %multiply_reduce_fusion = bf16[128,2048]{1,0:T(8,128)(2,1)} fusion(f32[128,2,2048]{2,1,0:T(2,128)S(1)} %reshape.355, f32[128,2]{1,0:T(8,128)S(1)} %copy-done.1), kind=kLoop, calls=%fused_computation.17 | loop fusion | flops 786432 | bytes 2622464 | tf_op jit(solution)/shard_map/reduce_sum | solution.py:138
  (16 shorter events, 0.2 us)
Async XLA Ops:
  182.5 5.2 %copy-start = (bf16[512,1,128]{2,0,1:T(8,128)(2,1)S(1)}, bf16[512,1,128]{2,0,1:T(8,128)(2,1)}, u32[]{:S(2)}) copy-start(bf16[512,1,128]{2,0,1:T(8,128)(2,1)} %param.11) | copy-start | bytes 393220
  182.5 62.9 %all-to-all-start.2 = ((bf16[4,320,2048]{2,1,0:T(8,128)(2,1)}), bf16[4,320,2048]{2,1,0:T(8,128)(2,1)}, u32[]{:S(2)}, u32[]{:S(2)}) async-start(bf16[4,320,2048]{2,1,0:T(8,128)(2,1)} %bitcast.85), calls=%async_computation.2 | async-start | bytes 10485760 | tf_op jit(solution)/shard_map/all_to_all | solution.py:25
  188.3 75.2 %collective-permute-start = (bf16[128,1,128]{2,0,1:T(8,128)(2,1)}, bf16[128,1,128]{2,0,1:T(8,128)(2,1)}, u32[]{:S(2)}, u32[]{:S(2)}) collective-permute-start(bf16[128,1,128]{2,0,1:T(8,128)(2,1)} %slice.18), channel_id=1, source_target_pairs={{0,4},{4,8},{8,12},{12,16},{16,20},{20,24},{24,28},{28,32},{32,36}... | collective-permute-start | bytes 98312 | tf_op jit(solution)/shard_map/ppermute | solution.py:15
  250.7 12.1 %copy-start.3 = (f32[128,2]{0,1:T(2,128)S(1)}, f32[128,2]{0,1:T(2,128)}, u32[]{:S(2)}) copy-start(f32[128,2]{0,1:T(2,128)} %param.16) | copy-start | bytes 3076
  250.7 60.6 %all-to-all-start.3 = ((bf16[64,5,2048]{2,1,0:T(8,128)(2,1)}), bf16[64,5,2048]{2,1,0:T(8,128)(2,1)S(1)}, u32[]{:S(2)}, u32[]{:S(2)}) async-start(bf16[64,5,2048]{2,1,0:T(8,128)(2,1)} %reshape.352), calls=%async_computation.3 | async-start | bytes 4194304 | tf_op jit(solution)/shard_map/all_to_all | solution.py:132
  260.4 7.9 %copy-start.2 = (f32[8]{0:T(128)S(1)}, f32[8]{0:T(128)}, u32[]{:S(2)}) copy-start(f32[8]{0:T(128)} %param.12) | copy-start | bytes 100
  311.9 4.7 %copy-start.1 = (f32[128,2]{1,0:T(8,128)S(1)}, f32[128,2]{1,0:T(8,128)}, u32[]{:S(2)}) copy-start(f32[128,2]{1,0:T(8,128)} %copy.41) | copy-start | bytes 3076
